TPU v7x, 32 devices: a whole 2x2x4 slice. The times are simulated.
32 devices in a mesh: ep: 4 (over y, x), tp: 8 (over z, core).
Axes of the slice: x: 2, y: 2, z: 4, core: 2. Of those that a mesh axis runs over, the one named last changes fastest.
Arguments:
- hidden_in: bfloat16 [128, 4096], P('ep'), may hold values from -6 to 6
- mix_gain: float32 [4096], replicated, may hold values from 0.1 to 1.9
- w_query: bfloat16 [4096, 2048], P('ep', 'tp'), may hold values from -0.09375 to 0.09375
- w_key: bfloat16 [4096, 2048], P('ep', 'tp'), may hold values from -0.09375 to 0.09375
- w_value: bfloat16 [4096, 2048], P('ep', 'tp'), may hold values from -0.09375 to 0.09375
- w_outgate: bfloat16 [4096, 2048], P('ep', 'tp'), may hold values from -0.09375 to 0.09375
- w_gates: bfloat16 [2, 4096, 32], P(None, None, 'tp'), may hold values from -0.09375 to 0.09375
- gate_bias: float32 [2, 32], P(None, 'tp'), may hold values from -1 to 4
- state_matrix: float32 [128, 32, 64, 64], P('ep', 'tp'), may hold values from -2 to 2
- state_norm: float32 [128, 32, 64], P('ep', 'tp'), may hold values from -2 to 2
- state_max: float32 [128, 32], P('ep', 'tp'), may hold values from -3 to 3
- w_mix_out: bfloat16 [2048, 4096], P('tp'), may hold values from -0.125 to 0.125
- ffn_gain: float32 [4096], replicated, may hold values from 0.1 to 1.9
- routes: int32 [128, 2], replicated, may hold values from 0 to 7, all different within a row; in each aligned block of 32 rows (0 to 31, 32 to 63, ...) at most 9 rows name the same one
- route_weights: float32 [128, 2], P('ep'), may hold values from 0.1 to 1
- expert_gate: bfloat16 [8, 4096, 2048], P('ep', None, 'tp'), may hold values from -0.09375 to 0.09375
- expert_up: bfloat16 [8, 4096, 2048], P('ep', None, 'tp'), may hold values from -0.09375 to 0.09375
- expert_down: bfloat16 [8, 2048, 4096], P('ep', 'tp'), may hold values from -0.125 to 0.125
- shared_gate: bfloat16 [4096, 1024], P(None, 'tp'), may hold values from -0.09375 to 0.09375
- shared_up: bfloat16 [4096, 1024], P(None, 'tp'), may hold values from -0.09375 to 0.09375
- shared_down: bfloat16 [1024, 4096], P('tp'), may hold values from -0.1875 to 0.1875
Outputs:
- result: bfloat16 [128, 4096], P('ep', 'tp')
- new_matrix: float32 [128, 32, 64, 64], P('ep', 'tp')
- new_norm: float32 [128, 32, 64], P('ep', 'tp')
- new_max: float32 [128, 32], P('ep', 'tp')
Inputs may be any that keep to these rules, and one draw needn't show every extreme that they name: `routes`: each row names 2 different experts. In each aligned block of 32 rows (the rows of one device group along ep) no expert is named by more than 9 rows, a bound that some block reaches.
All inputs are finite; a program needn't handle non-finite values.
Results may differ from a plain program's by a relative error of at most 0.023.
Values may be sent and summed in bfloat16 or wider, within the bound.
A program may use at most 64 MiB of HBM per device.

v0:
```python
import jax
import jax.numpy as jnp
from jax import lax
from jax.sharding import PartitionSpec as P

norm_eps = 1e-06


def rms_scale(inputs, scales):
    floats = inputs.astype(jnp.float32)
    return floats * lax.rsqrt(jnp.mean(floats * floats, -1, keepdims=True) + norm_eps) * scales


def slot_ranks(chosen, experts):
    flat_ids = chosen.reshape(-1)
    onehot = (flat_ids[:, None] == jnp.arange(experts, dtype=jnp.int32)[None, :]).astype(jnp.int32)
    earlier = jnp.cumsum(onehot, 0) - onehot
    return jnp.sum(earlier * onehot, 1).reshape(chosen.shape)


def per_device(
    hidden_in,
    mix_gain,
    w_query,
    w_key,
    w_value,
    w_outgate,
    w_gates,
    gate_bias,
    state_matrix,
    state_norm,
    state_max,
    w_mix_out,
    ffn_gain,
    routes,
    route_weights,
    expert_gate,
    expert_up,
    expert_down,
    shared_gate,
    shared_up,
    shared_down,
):
    ep_count = lax.axis_size("ep")
    tp_count = lax.axis_size("tp")
    group_index = lax.axis_index("ep")
    column_index = lax.axis_index("tp")
    seq_rows, width = hidden_in.shape
    heads_dev = state_matrix.shape[1]
    head_dim = state_matrix.shape[2]
    top_count = routes.shape[1]
    local_experts = expert_gate.shape[0]
    expert_total = local_experts * ep_count
    capacity = max(2, seq_rows * top_count // expert_total + 1)
    slot_count = ep_count * capacity
    slice_width = width // tp_count
    normed = rms_scale(hidden_in, mix_gain).astype(jnp.bfloat16)
    gathered = lax.all_to_all(normed, "ep", split_axis=1, concat_axis=0, tiled=True)
    joined = jnp.concatenate([w_query, w_key, w_value, w_outgate], 1)
    projected = lax.psum_scatter(
        jnp.dot(gathered, joined, preferred_element_type=jnp.float32).astype(jnp.bfloat16),
        "ep",
        scatter_dimension=0,
        tiled=True,
    )
    head_cols = heads_dev * head_dim

    def heads_of(role_index):
        part = projected[:, role_index * head_cols : (role_index + 1) * head_cols]
        return part.astype(jnp.float32).reshape(seq_rows, heads_dev, head_dim)

    query_heads = heads_of(0)
    key_heads = heads_of(1) * head_dim ** (-0.5)
    value_heads = heads_of(2)
    out_gate = heads_of(3)
    gate_pre = jnp.einsum("sd,gdh->gsh", normed, w_gates, preferred_element_type=jnp.float32)
    gate_pre = gate_pre + gate_bias[:, None, :]
    carried = jax.nn.log_sigmoid(gate_pre[1]) + state_max
    new_max = jnp.maximum(carried, gate_pre[0])
    forget_weight = jnp.exp(carried - new_max)[..., None]
    input_weight = jnp.exp(gate_pre[0] - new_max)[..., None]
    new_norm = forget_weight * state_norm + input_weight * key_heads
    new_matrix = (
        forget_weight[..., None] * state_matrix
        + (input_weight * value_heads)[..., :, None] * key_heads[..., None, :]
    )
    numerator = jnp.einsum(
        "shek,shk->she", new_matrix, query_heads, precision=lax.Precision.HIGHEST
    )
    denominator = jnp.maximum(jnp.abs(jnp.sum(new_norm * query_heads, -1)), 1.0)
    gated_out = (jax.nn.sigmoid(out_gate) * numerator / denominator[..., None]).reshape(
        seq_rows, head_cols
    )
    gated_out = gated_out.astype(jnp.bfloat16)
    mixed_part = jnp.dot(gated_out, w_mix_out, preferred_element_type=jnp.float32)
    mixed_own = lax.psum_scatter(
        mixed_part.astype(jnp.bfloat16), "tp", scatter_dimension=1, tiled=True
    ).astype(jnp.float32)
    residual_own = lax.dynamic_slice_in_dim(hidden_in, column_index * slice_width, slice_width, 1)
    stream_own = (residual_own.astype(jnp.float32) + mixed_own).astype(jnp.bfloat16)
    stream = lax.all_gather(stream_own, "tp", axis=1, tiled=True)
    ffn_in = rms_scale(stream, ffn_gain).astype(jnp.bfloat16)
    shared_hidden = (
        jax.nn.silu(jnp.dot(ffn_in, shared_gate, preferred_element_type=jnp.float32))
        * jnp.dot(ffn_in, shared_up, preferred_element_type=jnp.float32)
    ).astype(jnp.bfloat16)
    shared_part = jnp.dot(shared_hidden, shared_down, preferred_element_type=jnp.float32)
    own_routes = lax.dynamic_slice_in_dim(routes, group_index * seq_rows, seq_rows, 0)
    slot_ids = own_routes * capacity + slot_ranks(own_routes, expert_total)
    slot_range = jnp.arange(expert_total * capacity, dtype=jnp.int32)
    matches = slot_ids[:, :, None] == slot_range[None, None, :]
    chooser = jnp.any(matches, 1).astype(jnp.bfloat16)
    outgoing = jnp.einsum("sj,sd->jd", chooser, ffn_in, preferred_element_type=jnp.float32)
    outgoing = outgoing.astype(jnp.bfloat16).reshape(expert_total, capacity, width)
    arrived = lax.all_to_all(outgoing, "ep", split_axis=0, concat_axis=1, tiled=True)
    gate_values = jnp.einsum(
        "erd,edf->erf", arrived, expert_gate, preferred_element_type=jnp.float32
    )
    up_values = jnp.einsum("erd,edf->erf", arrived, expert_up, preferred_element_type=jnp.float32)
    expert_hidden = (jax.nn.silu(gate_values) * up_values).astype(jnp.bfloat16)
    expert_part = jnp.einsum(
        "erf,efd->erd", expert_hidden, expert_down, preferred_element_type=jnp.float32
    )
    expert_part = expert_part.reshape(local_experts * slot_count, width)
    routed_sum, shared_sum = (
        lax.psum_scatter(
            expert_part.astype(jnp.bfloat16), "tp", scatter_dimension=1, tiled=True
        ).astype(jnp.float32),
        lax.psum_scatter(
            shared_part.astype(jnp.bfloat16), "tp", scatter_dimension=1, tiled=True
        ).astype(jnp.float32),
    )
    expert_rows = routed_sum.astype(jnp.bfloat16)
    returned = lax.all_to_all(
        expert_rows.reshape(local_experts, slot_count, slice_width),
        "ep",
        split_axis=1,
        concat_axis=0,
        tiled=True,
    )
    returned = returned.reshape(expert_total * capacity, slice_width)
    weights = jnp.sum(jnp.where(matches, route_weights[:, :, None], 0.0), 1)
    routed = jnp.dot(weights, returned.astype(jnp.float32), precision=lax.Precision.HIGHEST)
    result = (stream_own.astype(jnp.float32) + shared_sum + routed).astype(jnp.bfloat16)
    return (result, new_matrix, new_norm, new_max)


def solution(mesh):
    placed = (
        P("ep", None),
        P(),
        P("ep", "tp"),
        P("ep", "tp"),
        P("ep", "tp"),
        P("ep", "tp"),
        P(None, None, "tp"),
        P(None, "tp"),
        P("ep", "tp", None, None),
        P("ep", "tp", None),
        P("ep", "tp"),
        P("tp", None),
        P(),
        P(),
        P("ep", None),
        P("ep", None, "tp"),
        P("ep", None, "tp"),
        P("ep", "tp", None),
        P(None, "tp"),
        P(None, "tp"),
        P("tp", None),
    )
    return jax.shard_map(
        per_device,
        mesh=mesh,
        in_specs=placed,
        out_specs=(P("ep", "tp"), P("ep", "tp", None, None), P("ep", "tp", None), P("ep", "tp")),
        check_vma=False,
    )
```

profile of v0, /device:TPU:0, one launch (start us, length us, event | category | flops | bytes accessed | tf_op | source)
XLA Modules:
  0.0 207.5 jit_solution(7990342096338553955)
XLA Ops:
  7.2 1.3 fusion.19
  8.4 1.1 fusion.21
  9.5 0.7 copy.88
  10.3 5.2 %all-to-all-start = ((bf16[32,4,1024]{2,0,1:T(8,128)(2,1)}), bf16[32,4,1024]{2,0,1:T(8,128)(2,1)S(1)}, u32[]{:S(2)}, u32[]{:S(2)}) async-start(bf16[32,4,1024]{2,0,1:T(8,128)(2,1)} %bitcast.53), calls=%async_computation | async-start | bytes 524288 | tf_op jit(solution)/shard_map/all_to_all | solution.py:58
  15.5 1.0 fusion.14
  16.5 4.3 %all-to-all-done = bf16[32,4,1024]{2,0,1:T(8,128)(2,1)S(1)} async-done(((bf16[32,4,1024]{2,0,1:T(8,128)(2,1)}), bf16[32,4,1024]{2,0,1:T(8,128)(2,1)S(1)}, u32[]{:S(2)}, u32[]{:S(2)}) %all-to-all-start) | async-done | bytes 262176 | tf_op jit(solution)/shard_map/all_to_all | solution.py:58
  20.8 2.7 %fusion.8 = bf16[128,1024]{1,0:T(8,128)(2,1)} fusion(bf16[128,1024]{1,0:T(8,128)(2,1)S(1)} %bitcast.60, bf16[1024,256]{1,0:T(8,128)(2,1)} %param.26, bf16[1024,256]{1,0:T(8,128)(2,1)} %param.25, bf16[1024,256]{1,0:T(8,128)(2,1)} %param.24, bf16[1024,256]{1,0:T(8,128)(2,1)} %param.23), kind=kOutput, calls=%fused_computation.13 | convolution fusion | flops 276955136 | bytes 2621440 | tf_op jit(solution)/shard_map/dot_general | solution.py:61
  24.2 23.9 %reduce-scatter.5.cloned.1.call-done = bf16[32,1024]{1,0:T(8,128)(2,1)} async-done(((bf16[128,1024]{1,0:T(8,128)(2,1)}), bf16[32,1024]{1,0:T(8,128)(2,1)}) %reduce-scatter.5.cloned.1.call-update) | async-done | bytes 65552 | tf_op jit(solution)/shard_map/reduce_scatter | solution.py:60
  48.1 0.8 fusion.54
  49.3 0.8 multiply_reduce_fusion
  50.1 0.7 add_divide_fusion
  50.9 3.7 %multiply_add_fusion = f32[32,4,64,64]{3,2,1,0:T(8,128)S(1)} fusion(f32[32,4,64,64]{3,2,1,0:T(8,128)} %param.29, f32[32,4,64]{2,1,0:T(4,128)S(1)} %get-tuple-element.9, f32[32,4,64]{2,1,0:T(4,128)S(1)} %get-tuple-element.13, f32[32,4]{1,0:T(8,128)S(1)} %copy.67), kind=kLoop, calls=%fused_computation.4 | loop fusion | flops 1572864 | bytes 4260352 | tf_op jit(solution)/shard_map/add | solution.py:84
  54.7 2.0 copy-done.1
  56.7 3.4 %fusion.55 = f32[32,4,1,64]{3,2,1,0:T(1,128)S(1)} fusion(f32[32,4,64,64]{3,2,1,0:T(8,128)S(1)} %multiply_add_fusion, bf16[32,4,64,1]{2,3,1,0:T(2,128)(2,1)S(1)} %reshape.111), kind=kOutput, calls=%fused_computation.85 | convolution fusion | flops 6291456 | bytes 2146304 | tf_op jit(solution)/shard_map/shek,shk->she/dot_general | solution.py:87
  60.3 1.2 convolution_convert_fusion.3
  62.1 30.2 %reduce-scatter.7.cloned.1.call-done = bf16[32,512]{1,0:T(8,128)(2,1)} async-done(((bf16[32,4096]{1,0:T(8,128)(2,1)}), bf16[32,512]{1,0:T(8,128)(2,1)}) %reduce-scatter.7.cloned.1.call-update) | async-done | bytes 32784 | tf_op jit(solution)/shard_map/reduce_scatter | solution.py:96
  92.3 0.8 add_convert_fusion
  93.1 14.2 %all_gather.3 = bf16[32,4096]{1,0:T(8,128)(2,1)S(1)} all-gather(bf16[32,512]{1,0:T(8,128)(2,1)S(1)} %add_convert_fusion), channel_id=1, replica_groups=mesh['ep'=4,'tp'=8] {'tp'}, dimensions={1}, use_global_device_ids=true | all-gather | bytes 294912 | tf_op jit(solution)/shard_map/all_gather | solution.py:101
  107.5 1.2 convolution_convert_fusion.1
  108.7 1.3 reshape.100
  110.0 18.2 %all_to_all.52 = bf16[8,9,4096]{2,1,0:T(8,128)(2,1)S(1)} all-to-all(bf16[8,9,4096]{2,1,0:T(8,128)(2,1)S(1)} %reshape.100), channel_id=1, replica_groups=mesh['ep'=4,'tp'=8] {'ep'}, dimensions={0} | all-to-all | bytes 1179648 | tf_op jit(solution)/shard_map/all_to_all | solution.py:115
  128.8 3.1 %fusion.17 = f32[2,36,256]{2,1,0:T(8,128)S(1)} fusion(bf16[2,4096,256]{2,1,0:T(8,128)(2,1)} %param.36, bf16[2,36,4096]{2,0,1:T(2,128)(2,1)S(1)} %bitcast.54), kind=kOutput, calls=%fused_computation.27 | convolution fusion | flops 150994944 | bytes 4857856 | tf_op jit(solution)/shard_map/erd,edf->erf/dot_general | solution.py:116
  131.9 6.0 %convolution_convert_fusion = bf16[2,36,4096]{2,1,0:T(8,128)(2,1)} fusion(bf16[2,256,4096]{2,1,0:T(8,128)(2,1)} %param.38, bf16[2,4096,256]{2,1,0:T(8,128)(2,1)} %param.37, bf16[2,36,4096]{2,0,1:T(2,128)(2,1)S(1)} %bitcast.55, f32[2,36,256]{2,1,0:T(8,128)S(1)} %fusion.17), kind=kOutput, calls=%fused_computation | convolution fusion | flops 302395392 | bytes 9641984 | tf_op jit(solution)/shard_map/erf,efd->erd/dot_general | solution.py:121
  137.9 2.0 convert_element_type.93
  140.0 1.6 fusion.51
  141.6 2.9 %convolution_convert_fusion.2 = bf16[32,4096]{1,0:T(8,128)(2,1)} fusion(bf16[128,4096]{1,0:T(8,128)(2,1)} %param.41, bf16[4096,128]{1,0:T(8,128)(2,1)} %param.40, f32[32,128]{1,0:T(8,128)S(1)} %fusion.51, bf16[32,4096]{1,0:T(8,128)(2,1)S(1)} %all_gather.3, f32[4096]{0:T(1024)S(1)} %copy-done.2, f32[32]{0:T(128)S(1)} %add_rsqrt_fusion), kind=kOutput, calls=%fused_computation.2 | convolution fusion | flops 67788800 | bytes 2654336 | tf_op jit(solution)/shard_map/dot_general | solution.py:107
  144.5 23.9 %reduce-scatter.11.cloned.1.call-done = bf16[72,512]{1,0:T(8,128)(2,1)} async-done(((bf16[72,4096]{1,0:T(8,128)(2,1)}), bf16[72,512]{1,0:T(8,128)(2,1)}) %reduce-scatter.11.cloned.1.call-update) | async-done | bytes 73744 | tf_op jit(solution)/shard_map/reduce_scatter | solution.py:126
  168.4 0.9 reshape.101
  170.0 3.6 %all-to-all-start.2 = ((bf16[2,36,512]{2,0,1:T(2,128)(2,1)}), bf16[2,36,512]{2,0,1:T(2,128)(2,1)S(1)}, u32[]{:S(2)}, u32[]{:S(2)}) async-start(bf16[2,36,512]{2,0,1:T(2,128)(2,1)} %copy.76), calls=%async_computation.6 | async-start | bytes 147456 | tf_op jit(solution)/shard_map/all_to_all | solution.py:134
  173.7 4.8 %all-to-all-done.2 = bf16[2,36,512]{2,0,1:T(2,128)(2,1)S(1)} async-done(((bf16[2,36,512]{2,0,1:T(2,128)(2,1)}), bf16[2,36,512]{2,0,1:T(2,128)(2,1)S(1)}, u32[]{:S(2)}, u32[]{:S(2)}) %all-to-all-start.2) | async-done | bytes 73760 | tf_op jit(solution)/shard_map/all_to_all | solution.py:134
  178.5 20.9 %reduce-scatter.9.cloned.1.call-done = bf16[32,512]{1,0:T(8,128)(2,1)} async-done(((bf16[32,4096]{1,0:T(8,128)(2,1)}), bf16[32,512]{1,0:T(8,128)(2,1)}) %reduce-scatter.9.cloned.1.call-update) | async-done | bytes 32784 | tf_op jit(solution)/shard_map/reduce_scatter | solution.py:129
  199.4 1.5 fusion.12
  (54 shorter events, 3.8 us)
Async XLA Ops:
  7.2 53.1 %copy-start = (bf16[256,4096]{1,0:T(8,128)(2,1)S(1)}, bf16[256,4096]{1,0:T(8,128)(2,1)}, u32[]{:S(2)}) copy-start(bf16[256,4096]{1,0:T(8,128)(2,1)} %param.32) | copy-start | bytes 6291460
  10.3 10.6 %all-to-all-start = ((bf16[32,4,1024]{2,0,1:T(8,128)(2,1)}), bf16[32,4,1024]{2,0,1:T(8,128)(2,1)S(1)}, u32[]{:S(2)}, u32[]{:S(2)}) async-start(bf16[32,4,1024]{2,0,1:T(8,128)(2,1)} %bitcast.53), calls=%async_computation | async-start | bytes 524288 | tf_op jit(solution)/shard_map/all_to_all | solution.py:58
  15.5 32.7 %reduce-scatter.5.cloned.1.call-start = ((), (), s32[]{:S(2)}) async-start(), calls=%async_computation.7 | async-start | bytes 327680 | tf_op jit(solution)/shard_map/reduce_scatter | solution.py:60
  16.5 7.1 %copy-start.4 = (f32[32,4]{0,1:T(4,128)S(1)}, f32[32,4]{0,1:T(4,128)}, u32[]{:S(2)}) copy-start(f32[32,4]{0,1:T(4,128)} %param.31) | copy-start | bytes 1540
  20.8 3.1 %copy-start.7 = (s32[128,2]{0,1:T(2,128)S(1)}, s32[128,2]{0,1:T(2,128)}, u32[]{:S(2)}) copy-start(s32[128,2]{0,1:T(2,128)} %param.34) | copy-start | bytes 3076
  20.8 28.4 %copy-start.3 = (f32[32,4,64]{2,1,0:T(4,128)S(1)}, f32[32,4,64]{2,1,0:T(4,128)}, u32[]{:S(2)}) copy-start(f32[32,4,64]{2,1,0:T(4,128)} %param.30) | copy-start | bytes 98308
  23.6 68.8 %reduce-scatter.7.cloned.1.call-start = ((), (), s32[]{:S(2)}) async-start(), calls=%async_computation.8 | async-start | bytes 294912 | tf_op jit(solution)/shard_map/reduce_scatter | solution.py:96
  23.6 31.0 %copy-start.5 = (f32[32,4]{0,1:T(4,128)}, f32[32,4]{0,1:T(4,128)S(1)}, u32[]{:S(2)}) copy-start(f32[32,4]{0,1:T(4,128)S(1)} %get-tuple-element.8) | copy-start | bytes 1540
  54.6 2.0 copy-start.1
  56.7 50.8 %copy-start.2 = (f32[4096]{0:T(1024)S(1)}, f32[4096]{0:T(1024)}, u32[]{:S(2)}) copy-start(f32[4096]{0:T(1024)} %param.33) | copy-start | bytes 49156
  61.4 106.9 %reduce-scatter.11.cloned.1.call-start = ((), (), s32[]{:S(2)}) async-start(), calls=%async_computation.10 | async-start | bytes 663552 | tf_op jit(solution)/shard_map/reduce_scatter | solution.py:126
  137.9 35.7 %copy-start.6 = (f32[32,2]{0,1:T(2,128)S(1)}, f32[32,2]{0,1:T(2,128)}, u32[]{:S(2)}) copy-start(f32[32,2]{0,1:T(2,128)} %param.35) | copy-start | bytes 772
  140.0 59.4 %reduce-scatter.9.cloned.1.call-start = ((), (), s32[]{:S(2)}) async-start(), calls=%async_computation.9 | async-start | bytes 294912 | tf_op jit(solution)/shard_map/reduce_scatter | solution.py:129
  170.0 8.5 %all-to-all-start.2 = ((bf16[2,36,512]{2,0,1:T(2,128)(2,1)}), bf16[2,36,512]{2,0,1:T(2,128)(2,1)S(1)}, u32[]{:S(2)}, u32[]{:S(2)}) async-start(bf16[2,36,512]{2,0,1:T(2,128)(2,1)} %copy.76), calls=%async_computation.6 | async-start | bytes 147456 | tf_op jit(solution)/shard_map/all_to_all | solution.py:134
Sparse Core Ops, SparseCore 0:
  23.7 24.3 reduce-scatter.4
  61.6 30.7 reduce-scatter.6
  140.1 28.2 reduce-scatter.10
  170.5 28.9 reduce-scatter.8
where the time goes:
time: 208 us
  waiting for transfers between devices  108 us (52%)
  blocking collectives  32.4 us (16%)
  matrix products  24.5 us (12%)
  between operations  14 us (7%)
  other arithmetic  10 us (5%)
  local copies, waits for them, and re-layouts  9.69 us (5%)
  starting transfers between devices  8.96 us (4%)
    reduce_scatter x1, waiting for transfers between devices, per_device(): lax.psum_scatter(mixed_part.astype(jnp.bfloat16), 'tp', scatter_dimension...  30.2 us
    reduce_scatter x1, waiting for transfers between devices, per_device(): lax.psum_scatter(jnp.dot(gathered, joined, preferred_element_type=jnp.flo...  23.9 us
    reduce_scatter x1, waiting for transfers between devices, per_device(): lax.psum_scatter(expert_part.astype(jnp.bfloat16), 'tp', scatter_dimensio...  23.9 us
    reduce_scatter x1, waiting for transfers between devices, per_device(): lax.psum_scatter(shared_part.astype(jnp.bfloat16), 'tp', scatter_dimensio...  20.9 us
    all_to_all x1, blocking collectives, per_device(): lax.all_to_all(outgoing, 'ep', split_axis=0, concat_axis=1, tiled=True)  18.2 us
    all_gather x1, blocking collectives, per_device(): stream = lax.all_gather(stream_own, 'tp', axis=1, tiled=True)  14.2 us
    dot_general x1, matrix products, per_device(): jnp.einsum('erf,efd->erd', expert_hidden, expert_down, preferred_element_...  6.02 us
    all_to_all x1, starting transfers between devices, per_device(): lax.all_to_all(normed, 'ep', split_axis=1, concat_axis=0, tiled=True)  5.19 us
  transfers between devices with their start and end apart: 6, of which 6 were waited for; matrix products, arithmetic and copies ran while one was open for 4% of the time, Pallas kernels for 0%

commit v1 on v0

--- a/solution.py
+++ b/solution.py
@@ -4,6 +4,17 @@
 from jax.sharding import PartitionSpec as P
 
 norm_eps = 1e-06
+
+
+def turned_line(x, axis, dim):
+    size = lax.axis_size(axis)
+    route = [(i, (i + 1) % size) for i in range(size)]
+    shards = [x]
+    for hop in range(1, size):
+        shards = [lax.ppermute(shards[0], axis, route), *shards]
+    full = jnp.concatenate(shards, axis=dim)
+    shift = (lax.axis_index(axis) + 1) * shards[-1].shape[dim]
+    return jnp.roll(full, shift, axis=dim)
 
 
 def rms_scale(inputs, scales):
@@ -98,7 +109,7 @@
     ).astype(jnp.float32)
     residual_own = lax.dynamic_slice_in_dim(hidden_in, column_index * slice_width, slice_width, 1)
     stream_own = (residual_own.astype(jnp.float32) + mixed_own).astype(jnp.bfloat16)
-    stream = lax.all_gather(stream_own, "tp", axis=1, tiled=True)
+    stream = turned_line(stream_own, "tp", 1)
     ffn_in = rms_scale(stream, ffn_gain).astype(jnp.bfloat16)
     shared_hidden = (
         jax.nn.silu(jnp.dot(ffn_in, shared_gate, preferred_element_type=jnp.float32))

time: 208 us -> 224 us (1.077)
  waiting for transfers between devices: 108 us -> 139 us
  blocking collectives: 32.4 us -> 24.6 us
  starting transfers between devices: 8.96 us -> 3.87 us
    ppermute x0 -> x7, waiting for transfers between devices: none -> 35 us  [turned_line(): shards = [lax.ppermute(shards[0], axis, route), *shards]]
    all_gather x1 -> x0, blocking collectives: 14.2 us -> none  [per_device(): stream = lax.all_gather(stream_own, 'tp', axis=1, tiled=True)]
    all_to_all x0 -> x1, blocking collectives: none -> 10.7 us  [per_device(): lax.all_to_all(normed, 'ep', split_axis=1, concat_axis=0, tiled=True)]
    all_to_all x1 -> x0, starting transfers between devices: 5.19 us -> none  [per_device(): lax.all_to_all(normed, 'ep', split_axis=1, concat_axis=0, tiled=True)]
    all_to_all x1, blocking collectives: 18.2 us -> 13.8 us  [per_device(): lax.all_to_all(outgoing, 'ep', split_axis=0, concat_axis=1, tiled=True)]
    all_to_all x1 -> x0, waiting for transfers between devices: 4.33 us -> none  [per_device(): lax.all_to_all(normed, 'ep', split_axis=1, concat_axis=0, tiled=True)]
  transfers between devices with their start and end apart: 6 -> 12, of which waited for: 6 -> 12; matrix products, arithmetic and copies ran while one was open for 4% -> 3% of each run, Pallas kernels for 0% -> 0%
where the time goes in v1:
time: 224 us; the launch traced here: 223 us
  waiting for transfers between devices  139 us (62%)
  blocking collectives  24.6 us (11%)
  matrix products  23.1 us (10%)
  between operations  14.1 us (6%)
  other arithmetic  10 us (4%)
  local copies, waits for them, and re-layouts  8.55 us (4%)
  starting transfers between devices  3.87 us (2%)
    ppermute x7, waiting for transfers between devices, turned_line(): shards = [lax.ppermute(shards[0], axis, route), *shards]  35 us
    reduce_scatter x1, waiting for transfers between devices, per_device(): lax.psum_scatter(mixed_part.astype(jnp.bfloat16), 'tp', scatter_dimension...  30.9 us
    reduce_scatter x1, waiting for transfers between devices, per_device(): lax.psum_scatter(expert_part.astype(jnp.bfloat16), 'tp', scatter_dimensio...  23.6 us
    reduce_scatter x1, waiting for transfers between devices, per_device(): lax.psum_scatter(jnp.dot(gathered, joined, preferred_element_type=jnp.flo...  23.6 us
    reduce_scatter x1, waiting for transfers between devices, per_device(): lax.psum_scatter(shared_part.astype(jnp.bfloat16), 'tp', scatter_dimensio...  20.9 us
    all_to_all x1, blocking collectives, per_device(): lax.all_to_all(outgoing, 'ep', split_axis=0, concat_axis=1, tiled=True)  13.8 us
    all_to_all x1, blocking collectives, per_device(): lax.all_to_all(normed, 'ep', split_axis=1, concat_axis=0, tiled=True)  10.7 us
    dot_general x1, matrix products, per_device(): jnp.einsum('erf,efd->erd', expert_hidden, expert_down, preferred_element_...  5.17 us
  transfers between devices with their start and end apart: 12, of which 12 were waited for; matrix products, arithmetic and copies ran while one was open for 3% of the time, Pallas kernels for 0%

profile of v1, /device:TPU:0, one launch (start us, length us, event | category | flops | bytes accessed | tf_op | source)
XLA Modules:
  0.0 223.0 jit_solution(13553378395084504847)
XLA Ops:
  7.2 1.2 fusion.19
  8.5 1.1 fusion.21
  9.6 10.7 %all_to_all.52 = bf16[32,4,1024]{2,0,1:T(8,128)(2,1)S(1)} all-to-all(bf16[32,4,1024]{2,0,1:T(8,128)(2,1)S(1)} %bitcast.58), channel_id=1, replica_groups=mesh['ep'=4,'tp'=8] {'ep'}, dimensions={1} | all-to-all | bytes 524288 | tf_op jit(solution)/shard_map/all_to_all | solution.py:69
  20.3 2.7 %fusion.8 = bf16[128,1024]{1,0:T(8,128)(2,1)} fusion(bf16[128,1024]{1,0:T(8,128)(2,1)S(1)} %bitcast.61, bf16[1024,256]{1,0:T(8,128)(2,1)} %param.26, bf16[1024,256]{1,0:T(8,128)(2,1)} %param.25, bf16[1024,256]{1,0:T(8,128)(2,1)} %param.24, bf16[1024,256]{1,0:T(8,128)(2,1)} %param.23), kind=kOutput, calls=%fused_computation.13 | convolution fusion | flops 276955136 | bytes 2621440 | tf_op jit(solution)/shard_map/dot_general | solution.py:72
  23.7 23.6 %reduce-scatter.5.cloned.1.call-done = bf16[32,1024]{1,0:T(8,128)(2,1)} async-done(((bf16[128,1024]{1,0:T(8,128)(2,1)}), bf16[32,1024]{1,0:T(8,128)(2,1)}) %reduce-scatter.5.cloned.1.call-update) | async-done | bytes 65552 | tf_op jit(solution)/shard_map/reduce_scatter | solution.py:71
  48.4 0.8 multiply_reduce_fusion
  50.0 3.7 %multiply_add_fusion = f32[32,4,64,64]{3,2,1,0:T(8,128)S(1)} fusion(f32[32,4,64,64]{3,2,1,0:T(8,128)} %param.29, f32[32,4,64]{2,1,0:T(4,128)S(1)} %get-tuple-element.9, f32[32,4,64]{2,1,0:T(4,128)S(1)} %get-tuple-element.13, f32[32,4]{1,0:T(8,128)S(1)} %copy.67), kind=kLoop, calls=%fused_computation.4 | loop fusion | flops 1572864 | bytes 4260352 | tf_op jit(solution)/shard_map/add | solution.py:95
  53.8 2.0 copy-done.1
  55.8 3.4 %fusion.55 = f32[32,4,1,64]{3,2,1,0:T(1,128)S(1)} fusion(f32[32,4,64,64]{3,2,1,0:T(8,128)S(1)} %multiply_add_fusion, bf16[32,4,64,1]{2,3,1,0:T(2,128)(2,1)S(1)} %reshape.111), kind=kOutput, calls=%fused_computation.101 | convolution fusion | flops 6291456 | bytes 2146304 | tf_op jit(solution)/shard_map/shek,shk->she/dot_general | solution.py:98
  59.4 1.2 convolution_convert_fusion.3
  60.6 30.9 %reduce-scatter.7.cloned.1.call-done = bf16[32,512]{1,0:T(8,128)(2,1)} async-done(((bf16[32,4096]{1,0:T(8,128)(2,1)}), bf16[32,512]{1,0:T(8,128)(2,1)}) %reduce-scatter.7.cloned.1.call-update) | async-done | bytes 32784 | tf_op jit(solution)/shard_map/reduce_scatter | solution.py:107
  92.4 5.1 %collective-permute-done = bf16[32,512]{1,0:T(8,128)(2,1)S(1)} collective-permute-done((bf16[32,512]{1,0:T(8,128)(2,1)S(1)}, bf16[32,512]{1,0:T(8,128)(2,1)S(1)}, u32[]{:S(2)}, u32[]{:S(2)}) %collective-permute-start) | collective-permute-done | bytes 32800 | tf_op jit(solution)/shard_map/ppermute | solution.py:14
  97.5 5.1 %collective-permute-done.1 = bf16[32,512]{1,0:T(8,128)(2,1)S(1)} collective-permute-done((bf16[32,512]{1,0:T(8,128)(2,1)S(1)}, bf16[32,512]{1,0:T(8,128)(2,1)S(1)}, u32[]{:S(2)}, u32[]{:S(2)}) %collective-permute-start.1) | collective-permute-done | bytes 32800 | tf_op jit(solution)/shard_map/ppermute | solution.py:14
  102.9 4.9 %collective-permute-done.2 = bf16[32,512]{1,0:T(8,128)(2,1)S(1)} collective-permute-done((bf16[32,512]{1,0:T(8,128)(2,1)S(1)}, bf16[32,512]{1,0:T(8,128)(2,1)S(1)}, u32[]{:S(2)}, u32[]{:S(2)}) %collective-permute-start.2) | collective-permute-done | bytes 32800 | tf_op jit(solution)/shard_map/ppermute | solution.py:14
  107.9 5.0 %collective-permute-done.3 = bf16[32,512]{1,0:T(8,128)(2,1)S(1)} collective-permute-done((bf16[32,512]{1,0:T(8,128)(2,1)S(1)}, bf16[32,512]{1,0:T(8,128)(2,1)S(1)}, u32[]{:S(2)}, u32[]{:S(2)}) %collective-permute-start.3) | collective-permute-done | bytes 32800 | tf_op jit(solution)/shard_map/ppermute | solution.py:14
  113.2 4.8 %collective-permute-done.4 = bf16[32,512]{1,0:T(8,128)(2,1)S(1)} collective-permute-done((bf16[32,512]{1,0:T(8,128)(2,1)S(1)}, bf16[32,512]{1,0:T(8,128)(2,1)S(1)}, u32[]{:S(2)}, u32[]{:S(2)}) %collective-permute-start.4) | collective-permute-done | bytes 32800 | tf_op jit(solution)/shard_map/ppermute | solution.py:14
  118.1 5.0 %collective-permute-done.5 = bf16[32,512]{1,0:T(8,128)(2,1)S(1)} collective-permute-done((bf16[32,512]{1,0:T(8,128)(2,1)S(1)}, bf16[32,512]{1,0:T(8,128)(2,1)S(1)}, u32[]{:S(2)}, u32[]{:S(2)}) %collective-permute-start.5) | collective-permute-done | bytes 32800 | tf_op jit(solution)/shard_map/ppermute | solution.py:14
  123.3 5.0 %collective-permute-done.6 = bf16[32,512]{1,0:T(8,128)(2,1)S(1)} collective-permute-done((bf16[32,512]{1,0:T(8,128)(2,1)S(1)}, bf16[32,512]{1,0:T(8,128)(2,1)S(1)}, u32[]{:S(2)}, u32[]{:S(2)}) %collective-permute-start.6) | collective-permute-done | bytes 32800 | tf_op jit(solution)/shard_map/ppermute | solution.py:14
  129.3 1.2 convolution_convert_fusion.1
  130.5 1.3 reshape.100
  131.8 13.8 %all_to_all.53 = bf16[8,9,4096]{2,1,0:T(8,128)(2,1)S(1)} all-to-all(bf16[8,9,4096]{2,1,0:T(8,128)(2,1)S(1)} %reshape.100), channel_id=1, replica_groups=mesh['ep'=4,'tp'=8] {'ep'}, dimensions={0} | all-to-all | bytes 1179648 | tf_op jit(solution)/shard_map/all_to_all | solution.py:126
  146.3 3.1 %fusion.17 = f32[2,36,256]{2,1,0:T(8,128)S(1)} fusion(bf16[2,4096,256]{2,1,0:T(8,128)(2,1)} %param.36, bf16[2,36,4096]{2,0,1:T(2,128)(2,1)S(1)} %bitcast.54), kind=kOutput, calls=%fused_computation.27 | convolution fusion | flops 150994944 | bytes 4857856 | tf_op jit(solution)/shard_map/erd,edf->erf/dot_general | solution.py:127
  149.4 5.2 %convolution_convert_fusion = bf16[2,36,4096]{2,1,0:T(8,128)(2,1)S(1)} fusion(bf16[2,256,4096]{2,1,0:T(8,128)(2,1)} %param.38, bf16[2,4096,256]{2,1,0:T(8,128)(2,1)} %param.37, bf16[2,36,4096]{2,0,1:T(2,128)(2,1)S(1)} %bitcast.55, f32[2,36,256]{2,1,0:T(8,128)S(1)} %fusion.17), kind=kOutput, calls=%fused_computation | convolution fusion | flops 302395392 | bytes 9641984 | tf_op jit(solution)/shard_map/erf,efd->erd/dot_general | solution.py:132
  154.6 0.9 convert_element_type.93
  155.6 1.6 fusion.51
  157.3 3.0 %convolution_convert_fusion.2 = bf16[32,4096]{1,0:T(8,128)(2,1)} fusion(bf16[128,4096]{1,0:T(8,128)(2,1)} %param.41, bf16[4096,128]{1,0:T(8,128)(2,1)} %param.40, f32[32,128]{1,0:T(8,128)S(1)} %fusion.51, f32[4096]{0:T(1024)S(1)} %copy-done.3, f32[32]{0:T(128)S(1)} %add_rsqrt_fusion, bf16[32,8192]{1,0:T(8,128)(2,1)} %copy-done.2, s32[]{:T(128)S(6)} %select_n.31), kind=kOutput, calls=%fused_computation.2 | convolution fusion | flops 67788800 | bytes 2654340 | tf_op jit(solution)/shard_map/dot_general | solution.py:118
  160.3 23.6 %reduce-scatter.11.cloned.1.call-done = bf16[72,512]{1,0:T(8,128)(2,1)} async-done(((bf16[72,4096]{1,0:T(8,128)(2,1)}), bf16[72,512]{1,0:T(8,128)(2,1)}) %reduce-scatter.11.cloned.1.call-update) | async-done | bytes 73744 | tf_op jit(solution)/shard_map/reduce_scatter | solution.py:137
  183.9 0.9 reshape.101
  185.5 3.6 %all-to-all-start.2 = ((bf16[2,36,512]{2,0,1:T(2,128)(2,1)}), bf16[2,36,512]{2,0,1:T(2,128)(2,1)S(1)}, u32[]{:S(2)}, u32[]{:S(2)}) async-start(bf16[2,36,512]{2,0,1:T(2,128)(2,1)} %copy.76), calls=%async_computation.6 | async-start | bytes 147456 | tf_op jit(solution)/shard_map/all_to_all | solution.py:145
  189.2 4.8 %all-to-all-done.2 = bf16[2,36,512]{2,0,1:T(2,128)(2,1)S(1)} async-done(((bf16[2,36,512]{2,0,1:T(2,128)(2,1)}), bf16[2,36,512]{2,0,1:T(2,128)(2,1)S(1)}, u32[]{:S(2)}, u32[]{:S(2)}) %all-to-all-start.2) | async-done | bytes 73760 | tf_op jit(solution)/shard_map/all_to_all | solution.py:145
  194.0 20.9 %reduce-scatter.9.cloned.1.call-done = bf16[32,512]{1,0:T(8,128)(2,1)} async-done(((bf16[32,4096]{1,0:T(8,128)(2,1)}), bf16[32,512]{1,0:T(8,128)(2,1)}) %reduce-scatter.9.cloned.1.call-update) | async-done | bytes 32784 | tf_op jit(solution)/shard_map/reduce_scatter | solution.py:140
  214.9 1.5 fusion.12
  (88 shorter events, 7.0 us)
Async XLA Ops:
  7.2 52.2 %copy-start = (bf16[256,4096]{1,0:T(8,128)(2,1)S(1)}, bf16[256,4096]{1,0:T(8,128)(2,1)}, u32[]{:S(2)}) copy-start(bf16[256,4096]{1,0:T(8,128)(2,1)} %param.32) | copy-start | bytes 6291460
  7.2 40.1 %reduce-scatter.5.cloned.1.call-start = ((), (), s32[]{:S(2)}) async-start(), calls=%async_computation.7 | async-start | bytes 327680 | tf_op jit(solution)/shard_map/reduce_scatter | solution.py:71
  20.3 2.8 %copy-start.9 = (bf16[2,4096,4]{1,2,0:T(4,128)(2,1)S(1)}, bf16[2,4096,4]{1,2,0:T(4,128)(2,1)}, u32[]{:S(2)}) copy-start(bf16[2,4096,4]{1,2,0:T(4,128)(2,1)} %param.27) | copy-start | bytes 196612
  20.3 2.8 %copy-start.10 = (f32[2,4]{1,0:T(2,128)S(1)}, f32[2,4]{1,0:T(2,128)}, u32[]{:S(2)}) copy-start(f32[2,4]{1,0:T(2,128)} %param.28) | copy-start | bytes 100
  20.3 3.0 %copy-start.5 = (f32[32,4]{0,1:T(4,128)S(1)}, f32[32,4]{0,1:T(4,128)}, u32[]{:S(2)}) copy-start(f32[32,4]{0,1:T(4,128)} %param.31) | copy-start | bytes 1540
  20.3 28.1 %copy-start.4 = (f32[32,4,64]{2,1,0:T(4,128)S(1)}, f32[32,4,64]{2,1,0:T(4,128)}, u32[]{:S(2)}) copy-start(f32[32,4,64]{2,1,0:T(4,128)} %param.30) | copy-start | bytes 98308
  23.1 68.4 %reduce-scatter.7.cloned.1.call-start = ((), (), s32[]{:S(2)}) async-start(), calls=%async_computation.8 | async-start | bytes 294912 | tf_op jit(solution)/shard_map/reduce_scatter | solution.py:107
  23.4 30.4 %copy-start.6 = (f32[32,4]{0,1:T(4,128)}, f32[32,4]{0,1:T(4,128)S(1)}, u32[]{:S(2)}) copy-start(f32[32,4]{0,1:T(4,128)S(1)} %get-tuple-element.8) | copy-start | bytes 1540
  53.8 2.0 copy-start.1
  55.8 46.8 %copy-start.8 = (s32[128,2]{0,1:T(2,128)S(1)}, s32[128,2]{0,1:T(2,128)}, u32[]{:S(2)}) copy-start(s32[128,2]{0,1:T(2,128)} %param.34) | copy-start | bytes 3076
  55.8 73.5 %copy-start.3 = (f32[4096]{0:T(1024)S(1)}, f32[4096]{0:T(1024)}, u32[]{:S(2)}) copy-start(f32[4096]{0:T(1024)} %param.33) | copy-start | bytes 49156
  60.6 123.3 %reduce-scatter.11.cloned.1.call-start = ((), (), s32[]{:S(2)}) async-start(), calls=%async_computation.10 | async-start | bytes 663552 | tf_op jit(solution)/shard_map/reduce_scatter | solution.py:137
  92.3 5.2 %collective-permute-start = (bf16[32,512]{1,0:T(8,128)(2,1)S(1)}, bf16[32,512]{1,0:T(8,128)(2,1)S(1)}, u32[]{:S(2)}, u32[]{:S(2)}) collective-permute-start(bf16[32,512]{1,0:T(8,128)(2,1)S(1)} %add_convert_fusion), channel_id=1, source_target_pairs={{0,1},{1,2},{2,3},{3,4},{4,5},{5,6},{6,7},{7,0},{8,9},{9,10},{10,1... | collective-permute-start | bytes 98312 | tf_op jit(solution)/shard_map/ppermute | solution.py:14
  97.5 5.1 %collective-permute-start.1 = (bf16[32,512]{1,0:T(8,128)(2,1)S(1)}, bf16[32,512]{1,0:T(8,128)(2,1)S(1)}, u32[]{:S(2)}, u32[]{:S(2)}) collective-permute-start(bf16[32,512]{1,0:T(8,128)(2,1)S(1)} %collective-permute-done), channel_id=1, source_target_pairs={{0,1},{1,2},{2,3},{3,4},{4,5},{5,6},{6,7},{7,0},{8,9},{9,10},{10,1... | collective-permute-start | bytes 98312 | tf_op jit(solution)/shard_map/ppermute | solution.py:14
  102.6 5.1 %collective-permute-start.2 = (bf16[32,512]{1,0:T(8,128)(2,1)S(1)}, bf16[32,512]{1,0:T(8,128)(2,1)S(1)}, u32[]{:S(2)}, u32[]{:S(2)}) collective-permute-start(bf16[32,512]{1,0:T(8,128)(2,1)S(1)} %collective-permute-done.1), channel_id=1, source_target_pairs={{0,1},{1,2},{2,3},{3,4},{4,5},{5,6},{6,7},{7,0},{8,9},{9,10},{10,1... | collective-permute-start | bytes 98312 | tf_op jit(solution)/shard_map/ppermute | solution.py:14
  107.8 5.1 %collective-permute-start.3 = (bf16[32,512]{1,0:T(8,128)(2,1)S(1)}, bf16[32,512]{1,0:T(8,128)(2,1)S(1)}, u32[]{:S(2)}, u32[]{:S(2)}) collective-permute-start(bf16[32,512]{1,0:T(8,128)(2,1)S(1)} %collective-permute-done.2), channel_id=1, source_target_pairs={{0,1},{1,2},{2,3},{3,4},{4,5},{5,6},{6,7},{7,0},{8,9},{9,10},{10,1... | collective-permute-start | bytes 98312 | tf_op jit(solution)/shard_map/ppermute | solution.py:14
  112.9 5.1 %collective-permute-start.4 = (bf16[32,512]{1,0:T(8,128)(2,1)S(1)}, bf16[32,512]{1,0:T(8,128)(2,1)S(1)}, u32[]{:S(2)}, u32[]{:S(2)}) collective-permute-start(bf16[32,512]{1,0:T(8,128)(2,1)S(1)} %collective-permute-done.3), channel_id=1, source_target_pairs={{0,1},{1,2},{2,3},{3,4},{4,5},{5,6},{6,7},{7,0},{8,9},{9,10},{10,1... | collective-permute-start | bytes 98312 | tf_op jit(solution)/shard_map/ppermute | solution.py:14
  118.1 5.1 %collective-permute-start.5 = (bf16[32,512]{1,0:T(8,128)(2,1)S(1)}, bf16[32,512]{1,0:T(8,128)(2,1)S(1)}, u32[]{:S(2)}, u32[]{:S(2)}) collective-permute-start(bf16[32,512]{1,0:T(8,128)(2,1)S(1)} %collective-permute-done.4), channel_id=1, source_target_pairs={{0,1},{1,2},{2,3},{3,4},{4,5},{5,6},{6,7},{7,0},{8,9},{9,10},{10,1... | collective-permute-start | bytes 98312 | tf_op jit(solution)/shard_map/ppermute | solution.py:14
  123.2 5.1 %collective-permute-start.6 = (bf16[32,512]{1,0:T(8,128)(2,1)S(1)}, bf16[32,512]{1,0:T(8,128)(2,1)S(1)}, u32[]{:S(2)}, u32[]{:S(2)}) collective-permute-start(bf16[32,512]{1,0:T(8,128)(2,1)S(1)} %collective-permute-done.5), channel_id=1, source_target_pairs={{0,1},{1,2},{2,3},{3,4},{4,5},{5,6},{6,7},{7,0},{8,9},{9,10},{10,1... | collective-permute-start | bytes 98312 | tf_op jit(solution)/shard_map/ppermute | solution.py:14
  128.5 0.8 copy-start.2
  154.6 34.5 %copy-start.7 = (f32[32,2]{0,1:T(2,128)S(1)}, f32[32,2]{0,1:T(2,128)}, u32[]{:S(2)}) copy-start(f32[32,2]{0,1:T(2,128)} %param.35) | copy-start | bytes 772
  155.5 59.4 %reduce-scatter.9.cloned.1.call-start = ((), (), s32[]{:S(2)}) async-start(), calls=%async_computation.9 | async-start | bytes 294912 | tf_op jit(solution)/shard_map/reduce_scatter | solution.py:140
  185.5 8.5 %all-to-all-start.2 = ((bf16[2,36,512]{2,0,1:T(2,128)(2,1)}), bf16[2,36,512]{2,0,1:T(2,128)(2,1)S(1)}, u32[]{:S(2)}, u32[]{:S(2)}) async-start(bf16[2,36,512]{2,0,1:T(2,128)(2,1)} %copy.76), calls=%async_computation.6 | async-start | bytes 147456 | tf_op jit(solution)/shard_map/all_to_all | solution.py:145
Sparse Core Ops, SparseCore 0:
  23.2 24.0 reduce-scatter.4
  60.7 30.7 reduce-scatter.6
  155.7 28.1 reduce-scatter.10
  186.0 28.8 reduce-scatter.8
